TPU v7x, 32 devices: a whole 2x2x4 slice. The times are simulated.
32 devices in a mesh: sp: 4 (over z), fs: 4 (over y, x), tp: 2 (over core).
Axes of the slice: x: 2, y: 2, z: 4, core: 2. Of those that a mesh axis runs over, the one named last changes fastest.
Arguments:
- tokens: bfloat16 [4, 1024, 2048], P('fs', 'sp', 'tp'), may hold values from -6 to 6
- norm_gain: float32 [2048], replicated, may hold values from 0.1 to 1.9
- ret_query: bfloat16 [2048, 1024], P('sp', 'tp'), may hold values from -0.125 to 0.125
- ret_key: bfloat16 [2048, 1024], P('sp', 'tp'), may hold values from -0.125 to 0.125
- ret_value: bfloat16 [2048, 1024], P('sp', 'tp'), may hold values from -0.125 to 0.125
- att_query: bfloat16 [2048, 1024], P('sp', 'tp'), may hold values from -0.125 to 0.125
- att_key: bfloat16 [2048, 256], P('sp', 'tp'), may hold values from -0.125 to 0.125
- att_value: bfloat16 [2048, 256], P('sp', 'tp'), may hold values from -0.125 to 0.125
- log_decay: float32 [4, 4, 1024], P('fs', 'tp', 'sp'), may hold values from -1 to 0
- start_state: float32 [4, 4, 256, 256], P('fs', 'tp'), may hold values from -12 to 12
- ret_gain: float32 [1024], P('tp'), may hold values from 0.1 to 1.9
- sink_logits: float32 [16], P('tp'), may hold values from 1 to 5
- ret_out: bfloat16 [1024, 2048], P('tp', 'fs'), may hold values from -0.1875 to 0.1875
- att_out: bfloat16 [1024, 2048], P('tp', 'fs'), may hold values from -1.5 to 1.5
Outputs:
- mixed: bfloat16 [4, 1024, 2048], P('fs', 'sp', 'tp')
All inputs are finite; a program needn't handle non-finite values.
Results may differ from a plain program's by a relative error of at most 0.015.
Values may be sent and summed in bfloat16 or wider, within the bound.
A program may use at most 128 MiB of HBM per device.

v0:
```python
import jax
import jax.numpy as jnp
from jax import lax
from jax.sharding import PartitionSpec as P

DK = 256
DV = 256
HD = 64
WINDOW = 128
BLOCK = 128
epsilon = 1e-06
exact_result = lax.Precision.HIGHEST


def carried_in(array, axis, combine, identity):
    peers, mine = (lax.axis_size(axis), lax.axis_index(axis))
    everything = jax.tree.map(
        lambda part, kind: lax.all_gather(part.astype(kind), axis),
        array,
        (jnp.bfloat16, jnp.bfloat16),
    )
    start = jax.tree.map(
        lambda part, zero: jnp.broadcast_to(jnp.asarray(zero, part.dtype), part.shape),
        array,
        identity,
    )

    def hop(k, before):
        reached = k < mine
        new = combine(
            before, jax.tree.map(lambda part, own: part[k].astype(own.dtype), everything, array)
        )
        return jax.tree.map(lambda a, b: jnp.where(reached, a, b), new, before)

    return lax.fori_loop(0, peers, hop, start)


def passed_along(block, axis, distance):
    devices = range(lax.axis_size(axis))
    route = [(i - distance, i) for i in devices if i - distance in devices]
    return lax.ppermute(block, axis, route)


def rotate(values, positions):
    half_dim = values.shape[-1] // 2
    inverse = 1.0 / 10000.0 ** (jnp.arange(half_dim, dtype=jnp.float32) / half_dim)
    angles = positions.astype(jnp.float32)[:, None] * inverse[None, :]
    cosine = jnp.cos(angles)[:, None, :]
    sine_table = jnp.sin(angles)[:, None, :]
    front_half = values[..., :half_dim]
    back_half = values[..., half_dim:]
    return jnp.concatenate(
        [
            front_half * cosine - back_half * sine_table,
            front_half * sine_table + back_half * cosine,
        ],
        axis=-1,
    )


def block_step(memory_state, inputs):
    queries, key_matrix_rows, value_matrix_rows, log_rates = inputs
    length_here = log_rates.shape[-1]
    causal = jnp.arange(length_here)[:, None] >= jnp.arange(length_here)[None, :]
    running_totals = jnp.cumsum(log_rates, axis=-1)
    relative = running_totals[:, :, None] - running_totals[:, None, :]
    weight = jnp.where(causal[None], jnp.exp(jnp.where(causal[None], relative, 0.0)), 0.0)
    score_matrix = (
        jnp.einsum("hqd,hkd->hqk", queries, key_matrix_rows, precision=exact_result) * weight
    )
    carried_state = jnp.einsum(
        "hqd,hdv->hqv",
        queries * jnp.exp(running_totals)[:, :, None],
        memory_state,
        precision=exact_result,
    )
    output_rows = (
        jnp.einsum("arf,afu->aru", score_matrix, value_matrix_rows, precision=exact_result)
        + carried_state
    )
    decay_factors = jnp.exp(running_totals[:, -1:] - running_totals)
    memory_state = memory_state * jnp.exp(running_totals[:, -1])[:, None, None] + jnp.einsum(
        "iwj,iwe->ije",
        key_matrix_rows * decay_factors[:, :, None],
        value_matrix_rows,
        precision=exact_result,
    )
    return (memory_state, output_rows)


def chain(earlier, later):
    return (earlier[0] * later[0], earlier[1] * later[0][:, None, None] + later[1])


def shards(
    tokens,
    norm_gain,
    ret_query,
    ret_key,
    ret_value,
    att_query,
    att_key,
    att_value,
    log_decay,
    start_state,
    ret_gain,
    sink_logits,
    ret_out,
    att_out,
):
    gathered = lax.all_gather(tokens[0], "tp", axis=1, tiled=True)
    row_count = gathered.shape[0]
    as_float = gathered.astype(jnp.float32)
    normed = (
        as_float
        * lax.rsqrt(jnp.mean(as_float * as_float, axis=-1, keepdims=True) + epsilon)
        * norm_gain
    ).astype(jnp.bfloat16)
    offset = lax.axis_index("sp") * row_count
    positions = offset + jnp.arange(row_count, dtype=jnp.int32)
    weights = (ret_query, ret_key, ret_value, att_query, att_key, att_value)
    pieces = (
        lax.all_gather(weights[0], "sp", axis=0, tiled=True),
        lax.all_gather(weights[1], "sp", axis=0, tiled=True),
        lax.all_gather(weights[2], "sp", axis=0, tiled=True),
        lax.all_gather(weights[3], "sp", axis=0, tiled=True),
        lax.all_gather(weights[4], "sp", axis=0, tiled=True),
        lax.all_gather(weights[5], "sp", axis=0, tiled=True),
    )
    projected = tuple(
        (jnp.dot(normed, piece, preferred_element_type=jnp.float32) for piece in pieces)
    )
    rounded = tuple((product_f.astype(jnp.bfloat16) for product_f in projected))
    projected = rounded[:3]
    head_count = projected[0].shape[1] // DK
    queries = rotate(projected[0].astype(jnp.float32).reshape(row_count, head_count, DK), positions)
    keys_rot = rotate(
        projected[1].astype(jnp.float32).reshape(row_count, head_count, DK), positions
    ) * DK ** (-0.5)
    values_f = projected[2].astype(jnp.float32).reshape(row_count, head_count, DV)
    log_rates = log_decay[0]
    count = row_count // BLOCK

    def blocked(array):
        return array.reshape(count, BLOCK, head_count, array.shape[-1]).transpose(0, 2, 1, 3)

    rates_blocked = log_rates.reshape(head_count, count, BLOCK).transpose(1, 0, 2)
    local_state, pieces = lax.scan(
        block_step,
        jnp.zeros((head_count, DK, DV), jnp.float32),
        (blocked(queries), blocked(keys_rot), blocked(values_f), rates_blocked),
    )
    local_out = pieces.transpose(0, 2, 1, 3).reshape(row_count, head_count, DV)
    running_totals = jnp.cumsum(log_rates, axis=-1)
    device_decay = jnp.exp(running_totals[:, -1])
    identity = (jnp.ones((head_count,), jnp.float32), jnp.zeros((head_count, DK, DV), jnp.float32))
    prior_decay, prior_state = carried_in((device_decay, local_state), "sp", chain, identity)
    incoming = prior_state + prior_decay[:, None, None] * start_state[0]
    retained = local_out + jnp.einsum(
        "thd,hdv->thv",
        queries * jnp.exp(running_totals).T[:, :, None],
        incoming,
        precision=exact_result,
    )
    centred = retained - jnp.mean(retained, axis=-1, keepdims=True)
    variance = jnp.mean(centred * centred, axis=-1, keepdims=True)
    ret_hidden = (
        (centred * lax.rsqrt(variance + epsilon)).reshape(row_count, head_count * DV) * ret_gain
    ).astype(jnp.bfloat16)
    att_queries, att_keys, att_values = rounded[3:]
    kv_heads = att_keys.shape[1] // HD
    groups = att_queries.shape[1] // HD // kv_heads
    earlier_keys, earlier_values = passed_along(
        (att_keys[row_count - WINDOW :], att_values[row_count - WINDOW :]), "sp", 1
    )
    extended_keys = jnp.concatenate([earlier_keys, att_keys], axis=0)
    extended_values = jnp.concatenate([earlier_values, att_values], axis=0)
    windows = row_count // WINDOW

    def banded(array):
        earlier = array[:row_count].reshape(windows, WINDOW, kv_heads, HD)
        current = array[WINDOW:].reshape(windows, WINDOW, kv_heads, HD)
        return jnp.concatenate([earlier, current], axis=1)

    key_band = banded(extended_keys)
    value_band = banded(extended_values)
    grouped_q = att_queries.reshape(windows, WINDOW, kv_heads, groups, HD)
    score_matrix = jnp.einsum(
        "nqhgd,nkhd->nhgqk", grouped_q, key_band, preferred_element_type=jnp.float32
    ) * HD ** (-0.5)
    query_index = WINDOW + jnp.arange(WINDOW)
    key_index = jnp.arange(2 * WINDOW)
    allowed = (key_index[None, :] <= query_index[:, None]) & (
        query_index[:, None] - key_index[None, :] < WINDOW
    )
    key_place = offset - WINDOW + jnp.arange(windows)[:, None] * WINDOW + key_index[None, :]
    visible = (allowed[None] & (key_place >= 0)[:, None, :])[:, None, None]
    expo = jnp.exp(jnp.where(visible, score_matrix, -1e30))
    summed = jnp.sum(expo, axis=-1, keepdims=True) + jnp.exp(sink_logits).reshape(
        1, kv_heads, groups, 1, 1
    )
    probs = (expo / summed).astype(jnp.bfloat16)
    attended = jnp.einsum(
        "nhgqk,nkhd->nqhgd", probs, value_band, preferred_element_type=jnp.float32
    )
    att_hidden = attended.astype(jnp.bfloat16).reshape(row_count, kv_heads * groups * HD)
    ret_width = ret_hidden.shape[1]
    joined = jnp.concatenate([ret_hidden, att_hidden], axis=1)[None]
    piece = lax.all_gather(joined, "fs", axis=0, tiled=True)
    product = jnp.einsum(
        "srh,hd->srd", piece[:, :, :ret_width], ret_out, preferred_element_type=jnp.float32
    )
    product = product + jnp.einsum(
        "srh,hd->srd", piece[:, :, ret_width:], att_out, preferred_element_type=jnp.float32
    )
    partial_rows = product.astype(jnp.bfloat16)
    regrouped = lax.all_to_all(partial_rows, "fs", split_axis=0, concat_axis=2, tiled=True)
    mixed = lax.psum_scatter(
        regrouped[0].astype(jnp.float32).astype(jnp.bfloat16), "tp", scatter_dimension=1, tiled=True
    )
    return mixed[None]


def solution(mesh):
    placed = (
        P("fs", "sp", "tp"),
        P(),
        P("sp", "tp"),
        P("sp", "tp"),
        P("sp", "tp"),
        P("sp", "tp"),
        P("sp", "tp"),
        P("sp", "tp"),
        P("fs", "tp", "sp"),
        P("fs", "tp", None, None),
        P("tp"),
        P("tp"),
        P("tp", "fs"),
        P("tp", "fs"),
    )
    return jax.shard_map(
        shards, mesh=mesh, in_specs=placed, out_specs=P("fs", "sp", "tp"), check_vma=False
    )
```

profile of v0, /device:TPU:0, one launch (start us, length us, event | category | flops | bytes accessed | tf_op | source)
XLA Modules:
  0.0 330.0 jit_solution(6295431087866726067)
XLA Ops:
  6.6 0.7 all-gather.20.cloned.1.call-update
  7.3 0.7 all-gather.12.cloned.1.call-update
  8.1 0.7 all-gather.16.cloned.1.call-update
  13.0 13.6 %all-reduce = bf16[8]{0:T(256)(128)(2,1)S(1)} all-reduce(bf16[8]{0:T(256)(128)(2,1)S(1)} %dynamic-update-slice), channel_id=3, replica_groups=mesh['sp'=4,'fs'=4,'tp'=2] {'sp'}, use_global_device_ids=true, to_apply=%add | all-reduce | flops 8 | bytes 32
  26.6 18.4 %all_gather.42 = bf16[2048,128]{1,0:T(8,128)(2,1)S(1)} all-gather(bf16[512,128]{1,0:T(8,128)(2,1)S(1)} %copy-done.12), channel_id=1, replica_groups=mesh['sp'=4,'fs'=4,'tp'=2] {'sp'}, dimensions={0}, use_global_device_ids=true | all-gather | bytes 655360 | tf_op jit(solution)/shard_map/all_gather | solution.py:127
  45.7 21.2 %all_gather.41 = bf16[2048,128]{1,0:T(8,128)(2,1)} all-gather(bf16[512,128]{1,0:T(8,128)(2,1)S(1)} %copy-done.13), channel_id=1, replica_groups=mesh['sp'=4,'fs'=4,'tp'=2] {'sp'}, dimensions={0}, use_global_device_ids=true | all-gather | bytes 655360 | tf_op jit(solution)/shard_map/all_gather | solution.py:128
  66.9 1.2 multiply_cosine_fusion
  68.1 0.8 broadcast_and_fusion
  68.9 1.6 fusion.25
  70.5 1.7 convolution_convert_fusion.5
  72.9 2.6 collective-permute-start.1
  75.5 5.5 %all-gather.12.cloned.1.call-done = bf16[2048,512]{1,0:T(8,128)(2,1)} async-done(((bf16[512,512]{1,0:T(8,128)(2,1)}), bf16[2048,512]{1,0:T(8,128)(2,1)}) %all-gather.12.cloned.1.call-update) | async-done | bytes 2097168 | tf_op jit(solution)/shard_map/all_gather | solution.py:124
  80.9 2.3 fusion.31
  83.6 44.0 %all-gather.16.cloned.1.call-done = bf16[2048,512]{1,0:T(8,128)(2,1)} async-done(((bf16[512,512]{1,0:T(8,128)(2,1)}), bf16[2048,512]{1,0:T(8,128)(2,1)}) %all-gather.16.cloned.1.call-update) | async-done | bytes 2097168 | tf_op jit(solution)/shard_map/all_gather | solution.py:123
  127.6 2.7 fusion.33
  130.3 1.1 reshape.299
  131.4 42.1 %all-gather.14.cloned.1.call-done = bf16[2048,512]{1,0:T(8,128)(2,1)} async-done(((bf16[512,512]{1,0:T(8,128)(2,1)}), bf16[2048,512]{1,0:T(8,128)(2,1)}) %all-gather.14.cloned.1.call-update) | async-done | bytes 2097168 | tf_op jit(solution)/shard_map/all_gather | solution.py:125
  173.6 2.7 fusion.32
  176.6 1.3 fusion.65
  178.9 6.7 %while.29 = (s32[]{:T(128)}, f32[2,256,256]{2,1,0:T(8,128)S(1)}, f32[2,2,128,256]{3,2,1,0:T(8,128)}, f32[2,2,128]{2,1,0:T(2,128)S(1)}, f32[2,2,128,256]{3,2,0,1:...) while((s32[]{:T(128)}, f32[2,256,256]{2,1,0:T(8,128)S(1)}, ...), condition=%wide.region_3.4_spmd.clone, body=%wide.region_1.3_spmd.clone.sunk | while | flops 604880896 | bytes 4242084 | solution.py:148
  180.2 1.2 fusion.95
  181.4 0.8 convolution_add_fusion.3
  183.6 1.2 fusion.95
  184.8 0.8 convolution_add_fusion.3
  185.6 0.7 convert_element_type.102
  186.4 1.9 convolution_convert_fusion.6
  188.6 2.3 collective-permute-start
  191.0 0.8 pad_maximum_fusion.2
  192.0 1.0 collective-permute-done
  193.2 1.3 copy.65
  194.9 24.5 %all-gather.18.cloned.1.call-done = bf16[2048,512]{1,0:T(8,128)(2,1)} async-done(((bf16[512,512]{1,0:T(8,128)(2,1)}), bf16[2048,512]{1,0:T(8,128)(2,1)}) %all-gather.18.cloned.1.call-update) | async-done | bytes 2097168 | tf_op jit(solution)/shard_map/all_gather | solution.py:126
  219.5 2.3 convolution_convert_fusion.1
  223.8 25.1 %all-gather.22.cloned.1.call-done = bf16[8,256,256]{2,1,0:T(8,128)(2,1)} async-done(((bf16[2,256,256]{2,1,0:T(8,128)(2,1)}), bf16[8,256,256]{2,1,0:T(8,128)(2,1)}) %all-gather.22.cloned.1.call-update) | async-done | bytes 1048592 | tf_op jit(solution)/shard_map/all_gather | solution.py:18
  248.9 4.6 %while.30 = (s32[]{:T(128)}, f32[2]{0:T(128)S(1)}, f32[2,256,256]{2,1,0:T(8,128)S(1)}, s32[]{:T(128)}, bf16[4,2]{1,0:T(4,128)(2,1)S(1)}, /*index=5*/bf16[4,2,256,256]{3,2,1,0:T(8,128)(2,1)}, s32[]{:T(128)}, s32[]{:T(128)}) while((s32[]{:T(128)}, f32[2]{0:T(128)S(1)}, f32[2,256,256]{2,1,0:T(8,128)S(1)}, s32[]{:T(128)}, ...), condition=%wide.region_7.8_spmd.clone, body=%wide.region_6.7_spmd.clone.sunk | while | flops 655372 | bytes 1310871 | solution.py:35
  248.9 1.2 fusion.96
  250.1 1.1 fusion.96
  251.3 1.1 fusion.96
  252.4 1.1 fusion.96
  253.6 1.2 fusion.67
  255.0 0.8 pad_maximum_fusion.1
  255.9 34.5 %all-gather.24.cloned.1.call-done = bf16[1024,1024]{0,1:T(8,128)(2,1)} async-done(((bf16[256,1024]{0,1:T(8,128)(2,1)}), bf16[1024,1024]{0,1:T(8,128)(2,1)}) %all-gather.24.cloned.1.call-update) | async-done | bytes 2097168 | tf_op jit(solution)/shard_map/all_gather | solution.py:209
  290.4 2.9 copy.81
  293.3 0.7 fusion.36
  294.4 0.7 add_convert_fusion
  295.1 16.7 %all_to_all.15 = bf16[4,256,512]{2,1,0:T(8,128)(2,1)S(1)} all-to-all(bf16[4,256,512]{2,1,0:T(8,128)(2,1)S(1)} %add_convert_fusion), channel_id=1, replica_groups=mesh['sp'=4,'fs'=4,'tp'=2] {'fs'}, dimensions={0} | all-to-all | bytes 2097152 | tf_op jit(solution)/shard_map/all_to_all | solution.py:217
  311.8 1.3 copy.82
  313.1 8.0 %reduce-scatter.2.cloned.1.call-done = bf16[256,1024]{0,1:T(8,128)(2,1)} async-done(((bf16[256,2048]{0,1:T(8,128)(2,1)}), bf16[256,1024]{0,1:T(8,128)(2,1)}) %reduce-scatter.2.cloned.1.call-update) | async-done | bytes 524304 | tf_op jit(solution)/shard_map/reduce_scatter | solution.py:218
  321.1 2.0 copy.83
  (138 shorter events, 13.2 us)
Async XLA Ops:
  6.5 286.8 %copy-start = (bf16[512,512]{1,0:T(8,128)(2,1)S(1)}, bf16[512,512]{1,0:T(8,128)(2,1)}, u32[]{:S(2)}) copy-start(bf16[512,512]{1,0:T(8,128)(2,1)} %param.30) | copy-start | bytes 1572868
  6.5 4.8 %copy-start.23 = (u32[32]{0:T(128)S(1)}, u32[32]{0:T(128)}, u32[]{:S(2)}) copy-start(u32[32]{0:T(128)} %constant.93) | copy-start | bytes 388
  6.5 3.5 %copy-start.15 = (f32[1,2,256]{2,1,0:T(2,128)S(1)}, f32[1,2,256]{2,1,0:T(2,128)}, u32[]{:S(2)}) copy-start(f32[1,2,256]{2,1,0:T(2,128)} %param.26) | copy-start | bytes 6148
  6.5 20.1 %copy-start.12 = (bf16[512,128]{1,0:T(8,128)(2,1)S(1)}, bf16[512,128]{1,0:T(8,128)(2,1)}, u32[]{:S(2)}) copy-start(bf16[512,128]{1,0:T(8,128)(2,1)} %param.24) | copy-start | bytes 393220
  6.5 38.6 %copy-start.22 = (f32[8]{0:T(128)S(1)}, f32[8]{0:T(128)}, u32[]{:S(2)}) copy-start(f32[8]{0:T(128)} %param.29) | copy-start | bytes 100
  6.5 39.2 %copy-start.13 = (bf16[512,128]{1,0:T(8,128)(2,1)S(1)}, bf16[512,128]{1,0:T(8,128)(2,1)}, u32[]{:S(2)}) copy-start(bf16[512,128]{1,0:T(8,128)(2,1)} %param.25) | copy-start | bytes 393220
  6.6 62.3 %all-gather.20.cloned.1.call-start = ((), (), s32[]{:S(2)}) async-start(), calls=%async_computation.7 | async-start | bytes 1572864 | tf_op jit(solution)/shard_map/all_gather | solution.py:111
  7.3 73.6 %all-gather.12.cloned.1.call-start = ((), (), s32[]{:S(2)}) async-start(), calls=%async_computation.2 | async-start | bytes 2621440 | tf_op jit(solution)/shard_map/all_gather | solution.py:124
  8.0 62.5 %copy-start.20 = (f32[2048]{0:T(1024)S(1)}, f32[2048]{0:T(1024)}, u32[]{:S(2)}) copy-start(f32[2048]{0:T(1024)} %param.19) | copy-start | bytes 24580
  8.1 119.6 %all-gather.16.cloned.1.call-start = ((), (), s32[]{:S(2)}) async-start(), calls=%async_computation.4 | async-start | bytes 2621440 | tf_op jit(solution)/shard_map/all_gather | solution.py:123
  8.8 164.8 %all-gather.14.cloned.1.call-start = ((), (), s32[]{:S(2)}) async-start(), calls=%async_computation.3 | async-start | bytes 2621440 | tf_op jit(solution)/shard_map/all_gather | solution.py:125
  9.4 210.1 %all-gather.18.cloned.1.call-start = ((), (), s32[]{:S(2)}) async-start(), calls=%async_computation.5 | async-start | bytes 2621440 | tf_op jit(solution)/shard_map/all_gather | solution.py:126
  10.0 238.9 %all-gather.22.cloned.1.call-start = ((), (), s32[]{:S(2)}) async-start(), calls=%async_computation.8 | async-start | bytes 1310720 | tf_op jit(solution)/shard_map/all_gather | solution.py:18
  68.9 12.1 %copy-start.5 = (bf16[1,256,2048]{2,1,0:T(8,128)(2,1)S(1)}, bf16[1,256,2048]{2,1,0:T(8,128)(2,1)}, u32[]{:S(2)}) copy-start(bf16[1,256,2048]{2,1,0:T(8,128)(2,1)} %all-gather.20.cloned.1.call-done) | copy-start | bytes 3145732
  70.5 103.1 %copy-start.18 = (f32[256]{0:T(256)}, f32[256]{0:T(256)S(1)}, u32[]{:S(2)}) copy-start(f32[256]{0:T(256)S(1)} %add_rsqrt_fusion.1) | copy-start | bytes 3076
  72.2 11.0 %copy-start.10 = (bf16[256,128]{1,0:T(8,128)(2,1)}, bf16[256,128]{1,0:T(8,128)(2,1)S(1)}, u32[]{:S(2)}) copy-start(bf16[256,128]{1,0:T(8,128)(2,1)S(1)} %convolution_convert_fusion.5) | copy-start | bytes 196612
  72.9 118.2 %collective-permute-start.1 = (bf16[128,128]{1,0:T(8,128)(2,1)}, bf16[128,128]{1,0:T(8,128)(2,1)}, u32[]{:S(2)}, u32[]{:S(2)}) collective-permute-start(bf16[128,128]{1,0:T(8,128)(2,1)} %slice.64), channel_id=1, source_target_pairs={{0,8},{8,16},{16,24},{1,9},{9,17},{17,25},{2,10},{10,18},{18,26},{... | collective-permute-start | bytes 98312 | tf_op jit(solution)/shard_map/ppermute | solution.py:41
  176.6 1.3 copy-start.8
  178.0 0.7 copy-start.3
  178.1 0.8 copy-start.1
  178.8 7.6 %copy-start.19 = (f32[256]{0:T(256)S(1)}, f32[256]{0:T(256)}, u32[]{:S(2)}) copy-start(f32[256]{0:T(256)} %copy-done.18) | copy-start | bytes 3076
  178.8 7.6 %copy-start.21 = (f32[2048]{0:T(1024)S(1)}, f32[2048]{0:T(1024)}, u32[]{:S(2)}) copy-start(f32[2048]{0:T(1024)} %param.19) | copy-start | bytes 24580
  185.6 2.7 copy-start.11
  186.4 104.1 %all-gather.24.cloned.1.call-start = ((), (), s32[]{:S(2)}) async-start(), calls=%async_computation.9 | async-start | bytes 2621440 | tf_op jit(solution)/shard_map/all_gather | solution.py:209
  188.3 31.2 %copy-start.6 = (bf16[1,256,2048]{2,1,0:T(8,128)(2,1)S(1)}, bf16[1,256,2048]{2,1,0:T(8,128)(2,1)}, u32[]{:S(2)}) copy-start(bf16[1,256,2048]{2,1,0:T(8,128)(2,1)} %all-gather.20.cloned.1.call-done) | copy-start | bytes 3145732
  188.6 4.3 %collective-permute-start = (bf16[128,128]{1,0:T(8,128)(2,1)S(1)}, bf16[128,128]{1,0:T(8,128)(2,1)S(1)}, u32[]{:S(2)}, u32[]{:S(2)}) collective-permute-start(bf16[128,128]{1,0:T(8,128)(2,1)S(1)} %slice.63), channel_id=1, source_target_pairs={{0,8},{8,16},{16,24},{1,9},{9,17},{17,25},{2,10},{10,18},{18,26},{... | collective-permute-start | bytes 98312 | tf_op jit(solution)/shard_map/ppermute | solution.py:41
  194.9 27.2 %copy-start.14 = (pred[2,128,256]{1,2,0:T(8,128)(4,1)S(1)}, pred[2,128,256]{1,2,0:T(8,128)(4,1)}, u32[]{:S(2)}) copy-start(pred[2,128,256]{1,2,0:T(8,128)(4,1)} %broadcast_and_fusion) | copy-start | bytes 196612
  221.8 1.0 copy-start.17
  248.9 4.6 %copy-start.2 = (f32[256,2,128]{2,0,1:T(8,128)S(1)}, f32[256,2,128]{2,0,1:T(8,128)}, u32[]{:S(2)}) copy-start(f32[256,2,128]{2,0,1:T(8,128)} %copy-done.1) | copy-start | bytes 786436
  248.9 4.6 %copy-start.4 = (f32[256,2,128]{2,0,1:T(8,128)S(1)}, f32[256,2,128]{2,0,1:T(8,128)}, u32[]{:S(2)}) copy-start(f32[256,2,128]{2,0,1:T(8,128)} %copy-done.3) | copy-start | bytes 786436
  248.9 4.6 %copy-start.9 = (f32[1,2,256,256]{3,2,1,0:T(8,128)S(1)}, f32[1,2,256,256]{3,2,1,0:T(8,128)}, u32[]{:S(2)}) copy-start(f32[1,2,256,256]{3,2,1,0:T(8,128)} %param.27) | copy-start | bytes 1572868
  253.5 1.3 copy-start.16
  255.9 65.2 %reduce-scatter.2.cloned.1.call-start = ((), (), s32[]{:S(2)}) async-start(), calls=%async_computation.6 | async-start | bytes 1572864 | tf_op jit(solution)/shard_map/reduce_scatter | solution.py:218
  293.3 1.0 copy-start.7
Sparse Core Ops, SparseCore 0:
  8.9 11.7 all-gather.19
  22.3 58.6 all-gather.11
  82.5 45.0 all-gather.15
  129.1 44.4 all-gather.13
  175.0 44.4 all-gather.17
  220.9 27.9 all-gather.21
  256.0 34.4 all-gather.23
  313.2 7.8 reduce-scatter.1
where the time goes:
time: 331 us; the launch traced here: 330 us
  waiting for transfers between devices  188 us (57%)
  blocking collectives  69.8 us (21%)
  matrix products  23 us (7%)
  local copies, waits for them, and re-layouts  16.4 us (5%)
  between operations  14.8 us (4%)
  other arithmetic  12.8 us (4%)
  starting transfers between devices  5.19 us (2%)
    all_gather x1, waiting for transfers between devices, shards(): lax.all_gather(weights[0], 'sp', axis=0, tiled=True)  44 us
    all_gather x1, waiting for transfers between devices, shards(): lax.all_gather(weights[2], 'sp', axis=0, tiled=True)  42.1 us
    all_gather x1, waiting for transfers between devices, shards(): piece = lax.all_gather(joined, 'fs', axis=0, tiled=True)  34.5 us
    all_gather x1, waiting for transfers between devices, carried_in(): lax.all_gather(part.astype(kind), axis)  25.1 us
    all_gather x1, waiting for transfers between devices, shards(): lax.all_gather(weights[3], 'sp', axis=0, tiled=True)  24.5 us
    all_gather x1, blocking collectives, shards(): lax.all_gather(weights[5], 'sp', axis=0, tiled=True)  21.2 us
    all_gather x1, blocking collectives, shards(): lax.all_gather(weights[4], 'sp', axis=0, tiled=True)  18.4 us
    all_to_all x1, blocking collectives, shards(): lax.all_to_all(partial_rows, 'fs', split_axis=0, concat_axis=2, tiled=True)  16.7 us
  transfers between devices with their start and end apart: 10, of which 8 were waited for; matrix products, arithmetic and copies ran while one was open for 11% of the time, Pallas kernels for 0%

commit v1 on v0

--- a/solution.py
+++ b/solution.py
@@ -119,8 +119,33 @@
     offset = lax.axis_index("sp") * row_count
     positions = offset + jnp.arange(row_count, dtype=jnp.int32)
     weights = (ret_query, ret_key, ret_value, att_query, att_key, att_value)
+
+    def list_the_streams(row_data, a_name):
+        g_now, answer, item_now = (lax.axis_size(a_name), lax.axis_index(a_name), row_data.shape[0])
+        stack_in = list(map(lambda w: (w, (w + 1) % g_now), range(g_now)))
+        sheets = list(map(lambda w: (w, (w - 1) % g_now), range(g_now)))
+        shaped = jnp.zeros(
+            (*row_data.shape[:0], g_now * item_now, *row_data.shape[1:]), row_data.dtype
+        )
+        arr_next = far_arr = row_data
+        shaped = lax.dynamic_update_slice_in_dim(shaped, row_data, answer * item_now, axis=0)
+        d = 1
+        a_now = g_now // 2
+        while d < a_now + 1:
+            arr_next = lax.ppermute(arr_next, a_name, stack_in)
+            shaped = lax.dynamic_update_slice_in_dim(
+                shaped, arr_next, (answer - d) % g_now * item_now, axis=0
+            )
+            if d < g_now - a_now:
+                far_arr = lax.ppermute(far_arr, a_name, sheets)
+                shaped = lax.dynamic_update_slice_in_dim(
+                    shaped, far_arr, (answer + d) % g_now * item_now, axis=0
+                )
+            d += 1
+        return shaped
+
     pieces = (
-        lax.all_gather(weights[0], "sp", axis=0, tiled=True),
+        list_the_streams(weights[0], "sp"),
         lax.all_gather(weights[1], "sp", axis=0, tiled=True),
         lax.all_gather(weights[2], "sp", axis=0, tiled=True),
         lax.all_gather(weights[3], "sp", axis=0, tiled=True),

time: 331 us -> 295 us (0.89)
  waiting for transfers between devices: 188 us -> 121 us
  blocking collectives: 69.8 us -> 85.1 us
  starting transfers between devices: 5.19 us -> 14.4 us
  local copies, waits for them, and re-layouts: 16.4 us -> 22.5 us
    all_gather x1 -> x0, waiting for transfers between devices: 44 us -> none  [shards(): lax.all_gather(weights[0], 'sp', axis=0, tiled=True)]
    all_gather x1, waiting for transfers between devices: 42.1 us -> 9.82 us  [shards(): lax.all_gather(weights[2], 'sp', axis=0, tiled=True)]
    ppermute x0 -> x3, waiting for transfers between devices: none -> 15.7 us  [the longest x2 15.7 us: list_the_streams(): arr_next = lax.ppermute(arr_next, a_name, stack_in)]
    unnamed x1, blocking collectives: 13.6 us -> 27.7 us
    ppermute x0 -> x3, starting transfers between devices: none -> 6.15 us  [the longest x2 4.06 us: list_the_streams(): arr_next = lax.ppermute(arr_next, a_name, stack_in)]
    all_gather x1, waiting for transfers between devices: 5.46 us -> 0.01 us  [shards(): lax.all_gather(weights[1], 'sp', axis=0, tiled=True)]
    dynamic_update_slice x0 -> x4, local copies, waits for them, and re-layouts: none -> 4.5 us  [the longest x1 1.91 us: list_the_streams(): lax.dynamic_update_slice_in_dim(shaped, far_arr, (answer + d) % g_now * i...]
  transfers between devices with their start and end apart: 10 -> 12, of which waited for: 8 -> 7; matrix products, arithmetic and copies ran while one was open for 11% -> 15% of each run, Pallas kernels for 0% -> 0%
where the time goes in v1:
time: 295 us; the launch traced here: 294 us
  waiting for transfers between devices  121 us (41%)
  blocking collectives  85.1 us (29%)
  matrix products  23 us (8%)
  local copies, waits for them, and re-layouts  22.5 us (8%)
  between operations  14.8 us (5%)
  starting transfers between devices  14.4 us (5%)
  other arithmetic  13.4 us (5%)
    all_gather x1, waiting for transfers between devices, shards(): piece = lax.all_gather(joined, 'fs', axis=0, tiled=True)  34.5 us
    unnamed x1, blocking collectives  27.7 us
    all_gather x1, waiting for transfers between devices, shards(): lax.all_gather(weights[3], 'sp', axis=0, tiled=True)  25.3 us
    all_gather x1, waiting for transfers between devices, carried_in(): lax.all_gather(part.astype(kind), axis)  24.6 us
    all_gather x1, blocking collectives, shards(): lax.all_gather(weights[4], 'sp', axis=0, tiled=True)  21.5 us
    all_gather x1, blocking collectives, shards(): lax.all_gather(weights[5], 'sp', axis=0, tiled=True)  19.2 us
    all_to_all x1, blocking collectives, shards(): lax.all_to_all(partial_rows, 'fs', split_axis=0, concat_axis=2, tiled=True)  16.7 us
    ppermute x2, waiting for transfers between devices, list_the_streams(): arr_next = lax.ppermute(arr_next, a_name, stack_in)  15.7 us
  transfers between devices with their start and end apart: 12, of which 7 were waited for; matrix products, arithmetic and copies ran while one was open for 15% of the time, Pallas kernels for 0%

profile of v1, /device:TPU:0, one launch (start us, length us, event | category | flops | bytes accessed | tf_op | source)
XLA Modules:
  0.0 294.3 jit_solution(2188932016409956058)
XLA Ops:
  8.8 3.1 %collective-permute-start = (bf16[512,512]{1,0:T(8,128)(2,1)}, bf16[512,512]{1,0:T(8,128)(2,1)S(1)}, u32[]{:S(2)}, u32[]{:S(2)}) collective-permute-start(bf16[512,512]{1,0:T(8,128)(2,1)} %param.20), channel_id=1, source_target_pairs={{0,8},{8,16},{16,24},{24,0},{1,9},{9,17},{17,25},{25,1},{2,10},{10... | collective-permute-start | bytes 1572872 | tf_op jit(solution)/shard_map/ppermute | solution.py:135
  11.9 2.1 collective-permute-start.1
  17.5 27.7 %all-reduce = bf16[8]{0:T(256)(128)(2,1)S(1)} all-reduce(bf16[8]{0:T(256)(128)(2,1)S(1)} %dynamic-update-slice), channel_id=3, replica_groups=mesh['sp'=4,'fs'=4,'tp'=2] {'sp'}, use_global_device_ids=true, to_apply=%add | all-reduce | flops 8 | bytes 32
  45.3 21.5 %all_gather.38 = bf16[2048,128]{1,0:T(8,128)(2,1)S(1)} all-gather(bf16[512,128]{1,0:T(8,128)(2,1)S(1)} %copy-done.13), channel_id=1, replica_groups=mesh['sp'=4,'fs'=4,'tp'=2] {'sp'}, dimensions={0}, use_global_device_ids=true | all-gather | bytes 655360 | tf_op jit(solution)/shard_map/all_gather | solution.py:152
  67.6 1.5 broadcast_in_dim.51
  69.2 0.9 constant_dynamic-update-slice_fusion.3
  70.0 0.8 broadcast_and_fusion
  70.8 19.2 %all_gather.37 = bf16[2048,128]{1,0:T(8,128)(2,1)} all-gather(bf16[512,128]{1,0:T(8,128)(2,1)S(1)} %copy-done.14), channel_id=1, replica_groups=mesh['sp'=4,'fs'=4,'tp'=2] {'sp'}, dimensions={0}, use_global_device_ids=true | all-gather | bytes 655360 | tf_op jit(solution)/shard_map/all_gather | solution.py:153
  90.0 1.2 multiply_cosine_fusion
  91.2 1.0 collective-permute-start.2
  92.2 0.9 constant_dynamic-update-slice_fusion.2
  93.0 1.9 constant_dynamic-update-slice_fusion.1
  95.0 1.7 fusion.25
  96.7 15.7 %collective-permute-done.2 = bf16[512,512]{1,0:T(8,128)(2,1)S(1)} collective-permute-done((bf16[512,512]{1,0:T(8,128)(2,1)S(1)}, bf16[512,512]{1,0:T(8,128)(2,1)S(1)}, u32[]{:S(2)}, u32[]{:S(2)}) %collective-permute-start.2) | collective-permute-done | bytes 524320 | tf_op jit(solution)/shard_map/ppermute | solution.py:135
  112.4 0.9 constant_dynamic-update-slice_fusion
  113.2 2.3 fusion.33
  115.9 1.7 convolution_convert_fusion.5
  118.3 6.4 %collective-permute-start.4 = (bf16[128,128]{1,0:T(8,128)(2,1)}, bf16[128,128]{1,0:T(8,128)(2,1)}, u32[]{:S(2)}, u32[]{:S(2)}) collective-permute-start(bf16[128,128]{1,0:T(8,128)(2,1)} %slice.64), channel_id=1, source_target_pairs={{0,8},{8,16},{16,24},{1,9},{9,17},{17,25},{2,10},{10,18},{18,26},{... | collective-permute-start | bytes 98312 | tf_op jit(solution)/shard_map/ppermute | solution.py:41
  124.7 2.7 fusion.31
  127.4 1.1 reshape.297
  128.5 9.8 %all-gather.13.cloned.1.call-done = bf16[2048,512]{1,0:T(8,128)(2,1)} async-done(((bf16[512,512]{1,0:T(8,128)(2,1)}), bf16[2048,512]{1,0:T(8,128)(2,1)}) %all-gather.13.cloned.1.call-update) | async-done | bytes 2097168 | tf_op jit(solution)/shard_map/all_gather | solution.py:150
  138.3 2.7 fusion.32
  141.4 1.3 fusion.65
  143.6 6.7 %while.29 = (s32[]{:T(128)}, f32[2,256,256]{2,1,0:T(8,128)S(1)}, f32[2,2,128,256]{3,2,1,0:T(8,128)}, f32[2,2,128]{2,1,0:T(2,128)S(1)}, f32[2,2,128,256]{3,2,0,1:...) while((s32[]{:T(128)}, f32[2,256,256]{2,1,0:T(8,128)S(1)}, ...), condition=%wide.region_3.4_spmd.clone, body=%wide.region_1.3_spmd.clone.sunk | while | flops 604880896 | bytes 4242084 | solution.py:173
  145.0 1.2 fusion.95
  146.2 0.8 convolution_add_fusion.3
  148.4 1.2 fusion.95
  149.6 0.8 convolution_add_fusion.3
  151.2 1.9 convolution_convert_fusion.6
  153.4 1.6 collective-permute-start.3
  156.1 1.0 collective-permute-done.3
  157.3 1.3 copy.65
  159.0 25.3 %all-gather.15.cloned.1.call-done = bf16[2048,512]{1,0:T(8,128)(2,1)} async-done(((bf16[512,512]{1,0:T(8,128)(2,1)}), bf16[2048,512]{1,0:T(8,128)(2,1)}) %all-gather.15.cloned.1.call-update) | async-done | bytes 2097168 | tf_op jit(solution)/shard_map/all_gather | solution.py:151
  184.3 2.3 convolution_convert_fusion.1
  188.6 24.6 %all-gather.19.cloned.1.call-done = bf16[8,256,256]{2,1,0:T(8,128)(2,1)} async-done(((bf16[2,256,256]{2,1,0:T(8,128)(2,1)}), bf16[8,256,256]{2,1,0:T(8,128)(2,1)}) %all-gather.19.cloned.1.call-update) | async-done | bytes 1048592 | tf_op jit(solution)/shard_map/all_gather | solution.py:18
  213.2 4.6 %while.30 = (s32[]{:T(128)}, f32[2]{0:T(128)S(1)}, f32[2,256,256]{2,1,0:T(8,128)S(1)}, s32[]{:T(128)}, bf16[4,2]{1,0:T(4,128)(2,1)S(1)}, /*index=5*/bf16[4,2,256,256]{3,2,1,0:T(8,128)(2,1)}, s32[]{:T(128)}, s32[]{:T(128)}) while((s32[]{:T(128)}, f32[2]{0:T(128)S(1)}, f32[2,256,256]{2,1,0:T(8,128)S(1)}, s32[]{:T(128)}, ...), condition=%wide.region_7.8_spmd.clone, body=%wide.region_6.7_spmd.clone.sunk | while | flops 655372 | bytes 1310871 | solution.py:35
  213.2 1.2 fusion.96
  214.4 1.1 fusion.96
  215.6 1.1 fusion.96
  216.7 1.1 fusion.96
  217.8 1.2 fusion.67
  219.3 0.8 pad_maximum_fusion.1
  220.2 34.5 %all-gather.21.cloned.1.call-done = bf16[1024,1024]{0,1:T(8,128)(2,1)} async-done(((bf16[256,1024]{0,1:T(8,128)(2,1)}), bf16[1024,1024]{0,1:T(8,128)(2,1)}) %all-gather.21.cloned.1.call-update) | async-done | bytes 2097168 | tf_op jit(solution)/shard_map/all_gather | solution.py:234
  254.7 2.9 copy.81
  259.4 16.7 %all_to_all.15 = bf16[4,256,512]{2,1,0:T(8,128)(2,1)S(1)} all-to-all(bf16[4,256,512]{2,1,0:T(8,128)(2,1)S(1)} %add_convert_fusion), channel_id=1, replica_groups=mesh['sp'=4,'fs'=4,'tp'=2] {'fs'}, dimensions={0} | all-to-all | bytes 2097152 | tf_op jit(solution)/shard_map/all_to_all | solution.py:242
  276.1 1.3 copy.82
  277.4 8.0 %reduce-scatter.2.cloned.1.call-done = bf16[256,1024]{0,1:T(8,128)(2,1)} async-done(((bf16[256,2048]{0,1:T(8,128)(2,1)}), bf16[256,1024]{0,1:T(8,128)(2,1)}) %reduce-scatter.2.cloned.1.call-update) | async-done | bytes 524304 | tf_op jit(solution)/shard_map/reduce_scatter | solution.py:243
  285.4 2.0 copy.83
  (150 shorter events, 17.6 us)
Async XLA Ops:
  6.5 251.1 %copy-start = (bf16[512,512]{1,0:T(8,128)(2,1)S(1)}, bf16[512,512]{1,0:T(8,128)(2,1)}, u32[]{:S(2)}) copy-start(bf16[512,512]{1,0:T(8,128)(2,1)} %param.30) | copy-start | bytes 1572868
  6.5 9.4 %copy-start.25 = (u32[32]{0:T(128)S(1)}, u32[32]{0:T(128)}, u32[]{:S(2)}) copy-start(u32[32]{0:T(128)} %constant.126) | copy-start | bytes 388
  6.5 7.7 %copy-start.16 = (f32[1,2,256]{2,1,0:T(2,128)S(1)}, f32[1,2,256]{2,1,0:T(2,128)}, u32[]{:S(2)}) copy-start(f32[1,2,256]{2,1,0:T(2,128)} %param.26) | copy-start | bytes 6148
  6.5 38.8 %copy-start.13 = (bf16[512,128]{1,0:T(8,128)(2,1)S(1)}, bf16[512,128]{1,0:T(8,128)(2,1)}, u32[]{:S(2)}) copy-start(bf16[512,128]{1,0:T(8,128)(2,1)} %param.24) | copy-start | bytes 393220
  6.5 60.4 %copy-start.24 = (f32[8]{0:T(128)S(1)}, f32[8]{0:T(128)}, u32[]{:S(2)}) copy-start(f32[8]{0:T(128)} %param.29) | copy-start | bytes 100
  6.5 88.4 %all-gather.17.cloned.1.call-start = ((), (), s32[]{:S(2)}) async-start(), calls=%async_computation.6 | async-start | bytes 1572864 | tf_op jit(solution)/shard_map/all_gather | solution.py:111
  7.3 117.4 %all-gather.11.cloned.1.call-start = ((), (), s32[]{:S(2)}) async-start(), calls=%async_computation.2 | async-start | bytes 2621440 | tf_op jit(solution)/shard_map/all_gather | solution.py:149
  8.0 61.1 %copy-start.9 = (bf16[512,512]{1,0:T(8,128)(2,1)S(1)}, bf16[512,512]{1,0:T(8,128)(2,1)}, u32[]{:S(2)}) copy-start(bf16[512,512]{1,0:T(8,128)(2,1)} %param.20) | copy-start | bytes 1572868
  8.0 130.3 %all-gather.13.cloned.1.call-start = ((), (), s32[]{:S(2)}) async-start(), calls=%async_computation.3 | async-start | bytes 2621440 | tf_op jit(solution)/shard_map/all_gather | solution.py:150
  8.8 175.5 %all-gather.15.cloned.1.call-start = ((), (), s32[]{:S(2)}) async-start(), calls=%async_computation.4 | async-start | bytes 2621440 | tf_op jit(solution)/shard_map/all_gather | solution.py:151
  8.8 82.4 %collective-permute-start = (bf16[512,512]{1,0:T(8,128)(2,1)}, bf16[512,512]{1,0:T(8,128)(2,1)S(1)}, u32[]{:S(2)}, u32[]{:S(2)}) collective-permute-start(bf16[512,512]{1,0:T(8,128)(2,1)} %param.20), channel_id=1, source_target_pairs={{0,8},{8,16},{16,24},{24,0},{1,9},{9,17},{17,25},{25,1},{2,10},{10... | collective-permute-start | bytes 1572872 | tf_op jit(solution)/shard_map/ppermute | solution.py:135
  11.9 81.1 %collective-permute-start.1 = (bf16[512,512]{1,0:T(8,128)(2,1)}, bf16[512,512]{1,0:T(8,128)(2,1)}, u32[]{:S(2)}, u32[]{:S(2)}) collective-permute-start(bf16[512,512]{1,0:T(8,128)(2,1)} %param.20), channel_id=1, source_target_pairs={{0,24},{8,0},{16,8},{24,16},{1,25},{9,1},{17,9},{25,17},{2,26},{10... | collective-permute-start | bytes 1572872 | tf_op jit(solution)/shard_map/ppermute | solution.py:140
  14.0 56.8 %copy-start.14 = (bf16[512,128]{1,0:T(8,128)(2,1)S(1)}, bf16[512,128]{1,0:T(8,128)(2,1)}, u32[]{:S(2)}) copy-start(bf16[512,128]{1,0:T(8,128)(2,1)} %param.25) | copy-start | bytes 393220
  14.1 199.1 %all-gather.19.cloned.1.call-start = ((), (), s32[]{:S(2)}) async-start(), calls=%async_computation.7 | async-start | bytes 1310720 | tf_op jit(solution)/shard_map/all_gather | solution.py:18
  66.8 23.2 %copy-start.18 = (f32[256]{0:T(256)S(1)}, f32[256]{0:T(256)}, u32[]{:S(2)}) copy-start(f32[256]{0:T(256)} %add_convert_fusion.1) | copy-start | bytes 3076
  91.2 22.1 %copy-start.22 = (f32[2048]{0:T(1024)S(1)}, f32[2048]{0:T(1024)}, u32[]{:S(2)}) copy-start(f32[2048]{0:T(1024)} %param.19) | copy-start | bytes 24580
  91.2 21.2 %collective-permute-start.2 = (bf16[512,512]{1,0:T(8,128)(2,1)S(1)}, bf16[512,512]{1,0:T(8,128)(2,1)S(1)}, u32[]{:S(2)}, u32[]{:S(2)}) collective-permute-start(bf16[512,512]{1,0:T(8,128)(2,1)S(1)} %collective-permute-done), channel_id=1, source_target_pairs={{0,8},{8,16},{16,24},{24,0},{1,9},{9,17},{17,25},{25,1},{2,10},{10... | collective-permute-start | bytes 1572872 | tf_op jit(solution)/shard_map/ppermute | solution.py:135
  95.0 18.3 %copy-start.5 = (bf16[1,256,2048]{2,1,0:T(8,128)(2,1)S(1)}, bf16[1,256,2048]{2,1,0:T(8,128)(2,1)}, u32[]{:S(2)}) copy-start(bf16[1,256,2048]{2,1,0:T(8,128)(2,1)} %all-gather.17.cloned.1.call-done) | copy-start | bytes 3145732
  96.7 41.7 %copy-start.20 = (f32[256]{0:T(256)}, f32[256]{0:T(256)S(1)}, u32[]{:S(2)}) copy-start(f32[256]{0:T(256)S(1)} %add_rsqrt_fusion.1) | copy-start | bytes 3076
  117.7 9.7 %copy-start.11 = (bf16[256,128]{1,0:T(8,128)(2,1)}, bf16[256,128]{1,0:T(8,128)(2,1)S(1)}, u32[]{:S(2)}) copy-start(bf16[256,128]{1,0:T(8,128)(2,1)S(1)} %convolution_convert_fusion.5) | copy-start | bytes 196612
  118.3 36.9 %collective-permute-start.4 = (bf16[128,128]{1,0:T(8,128)(2,1)}, bf16[128,128]{1,0:T(8,128)(2,1)}, u32[]{:S(2)}, u32[]{:S(2)}) collective-permute-start(bf16[128,128]{1,0:T(8,128)(2,1)} %slice.64), channel_id=1, source_target_pairs={{0,8},{8,16},{16,24},{1,9},{9,17},{17,25},{2,10},{10,18},{18,26},{... | collective-permute-start | bytes 98312 | tf_op jit(solution)/shard_map/ppermute | solution.py:41
  141.4 1.3 copy-start.8
  142.8 0.7 copy-start.3
  142.8 0.8 copy-start.1
  143.6 7.6 %copy-start.21 = (f32[256]{0:T(256)S(1)}, f32[256]{0:T(256)}, u32[]{:S(2)}) copy-start(f32[256]{0:T(256)} %copy-done.20) | copy-start | bytes 3076
  143.6 7.6 %copy-start.23 = (f32[2048]{0:T(1024)S(1)}, f32[2048]{0:T(1024)}, u32[]{:S(2)}) copy-start(f32[2048]{0:T(1024)} %param.19) | copy-start | bytes 24580
  150.4 2.7 copy-start.12
  151.1 103.6 %all-gather.21.cloned.1.call-start = ((), (), s32[]{:S(2)}) async-start(), calls=%async_computation.8 | async-start | bytes 2621440 | tf_op jit(solution)/shard_map/all_gather | solution.py:234
  153.1 31.2 %copy-start.6 = (bf16[1,256,2048]{2,1,0:T(8,128)(2,1)S(1)}, bf16[1,256,2048]{2,1,0:T(8,128)(2,1)}, u32[]{:S(2)}) copy-start(bf16[1,256,2048]{2,1,0:T(8,128)(2,1)} %all-gather.17.cloned.1.call-done) | copy-start | bytes 3145732
  153.4 3.7 %collective-permute-start.3 = (bf16[128,128]{1,0:T(8,128)(2,1)S(1)}, bf16[128,128]{1,0:T(8,128)(2,1)S(1)}, u32[]{:S(2)}, u32[]{:S(2)}) collective-permute-start(bf16[128,128]{1,0:T(8,128)(2,1)S(1)} %slice.63), channel_id=1, source_target_pairs={{0,8},{8,16},{16,24},{1,9},{9,17},{17,25},{2,10},{10,18},{18,26},{... | collective-permute-start | bytes 98312 | tf_op jit(solution)/shard_map/ppermute | solution.py:41
  159.0 27.9 %copy-start.15 = (pred[2,128,256]{1,2,0:T(8,128)(4,1)S(1)}, pred[2,128,256]{1,2,0:T(8,128)(4,1)}, u32[]{:S(2)}) copy-start(pred[2,128,256]{1,2,0:T(8,128)(4,1)} %broadcast_and_fusion) | copy-start | bytes 196612
  186.6 1.0 copy-start.19
  213.2 4.6 %copy-start.2 = (f32[256,2,128]{2,0,1:T(8,128)S(1)}, f32[256,2,128]{2,0,1:T(8,128)}, u32[]{:S(2)}) copy-start(f32[256,2,128]{2,0,1:T(8,128)} %copy-done.1) | copy-start | bytes 786436
  213.2 4.6 %copy-start.4 = (f32[256,2,128]{2,0,1:T(8,128)S(1)}, f32[256,2,128]{2,0,1:T(8,128)}, u32[]{:S(2)}) copy-start(f32[256,2,128]{2,0,1:T(8,128)} %copy-done.3) | copy-start | bytes 786436
  213.2 4.6 %copy-start.10 = (f32[1,2,256,256]{3,2,1,0:T(8,128)S(1)}, f32[1,2,256,256]{3,2,1,0:T(8,128)}, u32[]{:S(2)}) copy-start(f32[1,2,256,256]{3,2,1,0:T(8,128)} %param.27) | copy-start | bytes 1572868
  217.8 1.3 copy-start.17
  220.2 65.2 %reduce-scatter.2.cloned.1.call-start = ((), (), s32[]{:S(2)}) async-start(), calls=%async_computation.5 | async-start | bytes 1572864 | tf_op jit(solution)/shard_map/reduce_scatter | solution.py:243
  257.6 1.0 copy-start.7
Sparse Core Ops, SparseCore 0:
  8.9 11.7 all-gather.16
  22.3 64.3 all-gather.10
  88.2 50.0 all-gather.12
  139.8 44.5 all-gather.14
  185.7 27.4 all-gather.18
  220.3 34.4 all-gather.20
  277.5 7.8 reduce-scatter.1
